TPU v7x, 32 devices: a whole 2x2x4 slice. The times are simulated.
32 devices in a mesh: sp: 16 (over z, y, x), tp: 2 (over core).
Axes of the slice: x: 2, y: 2, z: 4, core: 2. Of those that a mesh axis runs over, the one named last changes fastest.
Arguments:
- tokens: bfloat16 [2048, 4096], P('sp'), may hold values from -6 to 6
- norm_gain: float32 [4096], replicated, may hold values from 0.1 to 1.9
- w_query: bfloat16 [4096, 2048], P('sp', 'tp'), may hold values from -1 to 1
- w_key: bfloat16 [4096, 512], P('sp', 'tp'), may hold values from -1 to 1
- w_value: bfloat16 [4096, 512], P('sp', 'tp'), may hold values from -0.09375 to 0.09375
- w_state_in: bfloat16 [4096, 2048], P('sp', 'tp'), may hold values from -0.09375 to 0.09375
- sink_logit: float32 [32], P('tp'), may hold values from 2 to 6
- decay_rate: float32 [128, 64], P('tp'), may hold values from 0.0002 to 4
- rotation: float32 [128, 64], P('tp'), may hold values from 1 to 60
- log_step: float32 [128], P('tp'), may hold values from -5.3 to -3
- in_re: float32 [128, 64, 16], P('tp'), may hold values from -1.5 to 1.5
- in_im: float32 [128, 64, 16], P('tp'), may hold values from -1.5 to 1.5
- out_re: float32 [128, 16, 64], P('tp'), may hold values from -0.75 to 0.75
- out_im: float32 [128, 16, 64], P('tp'), may hold values from -0.75 to 0.75
- skip_gain: float32 [2048], P('tp'), may hold values from -4 to 4
- w_attn_out: bfloat16 [2048, 4096], P('tp', 'sp'), may hold values from -0.5 to 0.5
- w_state_out: bfloat16 [2048, 4096], P('tp', 'sp'), may hold values from -0.125 to 0.125
- out_gain: float32 [4096], replicated, may hold values from 0.1 to 1.9
Outputs:
- mixed: bfloat16 [2048, 4096], P(('sp', 'tp'))
All inputs are finite; a program needn't handle non-finite values.
Results may differ from a plain program's by a relative error of at most 0.015.
The roundings to bfloat16 on the way count: a program that leaves them out, or rounds other values in their place, can miss the bound.
Values may be sent and summed in bfloat16 or wider, within the bound.
No kernel may reach another device: no remote copies, remote signals or barrier semaphores. Data moves between devices by JAX's collectives and lax.ppermute only.
A program may use at most 128 MiB of HBM per device.

v0:
```python
import math
import jax
import jax.numpy as jnp
from jax import lax
from jax.sharding import PartitionSpec as P

HEAD = 64
WINDOW = 128
epsilon = 1e-06
rotary_base = 500000.0


def carried_in(value, axis, join, neutral):
    count, mine = (lax.axis_size(axis), lax.axis_index(axis))
    pieces = jax.tree.map(lambda part: lax.all_gather(part, axis), value)
    so_far = jax.tree.map(
        lambda part, zero: jnp.full_like(part, 0) + jnp.asarray(zero, part.dtype), value, neutral
    )

    def turn(position, so_far):
        longer = join(so_far, jax.tree.map(lambda part: part[position], pieces))
        return jax.tree.map(lambda new, old: jnp.where(position < mine, new, old), longer, so_far)

    return lax.fori_loop(0, count - 1, turn, so_far)


def passed_along(value, axis, by):
    size = lax.axis_size(axis)
    pairs = [(i, i + by) for i in range(size) if 0 <= i + by < size]
    return lax.ppermute(value, axis, pairs)


def rotate(heads_block, positions):
    head_width = heads_block.shape[-1]
    half_width = head_width // 2
    frequency = rotary_base ** (-(jnp.arange(half_width, dtype=jnp.float32) * 2.0 / head_width))
    angles = positions.astype(jnp.float32)[:, None] * frequency[None, :]
    cosine = jnp.cos(angles)[:, None, :]
    sine_part = jnp.sin(angles)[:, None, :]
    lower_half = heads_block[..., :half_width]
    upper_half = heads_block[..., half_width:]
    return jnp.concatenate(
        [
            lower_half * cosine - upper_half * sine_part,
            upper_half * cosine + lower_half * sine_part,
        ],
        axis=-1,
    )


def shape_heads(query_sum, key_sum, value_sum, positions, head_width):
    row_count = query_sum.shape[0]
    kv_heads = key_sum.shape[1] // head_width
    group_size = query_sum.shape[1] // key_sum.shape[1]
    queries = rotate(
        query_sum.reshape(row_count, kv_heads * group_size, head_width), positions
    ).astype(jnp.bfloat16)
    queries = queries.reshape(row_count, kv_heads, group_size, head_width)
    key_rows = rotate(key_sum.reshape(row_count, kv_heads, head_width), positions).astype(
        jnp.bfloat16
    )
    key_rows = key_rows.reshape(row_count, kv_heads * head_width)
    value_rows = value_sum.astype(jnp.bfloat16)
    return (queries, key_rows, value_rows)


def band_attention(queries, key_rows, value_rows, sink_logit, first_row, window):
    row_count, kv_heads, group_size, head_width = queries.shape
    blocks = row_count // window
    query_blocks = queries.reshape(blocks, window, kv_heads, group_size, head_width)
    key_blocks = jnp.concatenate(
        [
            key_rows[:row_count].reshape(blocks, window, kv_heads, head_width),
            key_rows[window:].reshape(blocks, window, kv_heads, head_width),
        ],
        axis=1,
    )
    value_blocks = jnp.concatenate(
        [
            value_rows[:row_count].reshape(blocks, window, kv_heads, head_width),
            value_rows[window:].reshape(blocks, window, kv_heads, head_width),
        ],
        axis=1,
    )
    scores = jnp.einsum(
        "bqkgd,bskd->bkgqs", query_blocks, key_blocks, preferred_element_type=jnp.float32
    ) / math.sqrt(head_width)
    block_start = jnp.arange(blocks, dtype=jnp.int32)[:, None, None] * window
    query_at = first_row + block_start + jnp.arange(window, dtype=jnp.int32)[None, :, None]
    key_at = (
        first_row - window + block_start + jnp.arange(2 * window, dtype=jnp.int32)[None, None, :]
    )
    offset_gap = query_at - key_at
    visible = (offset_gap >= 0) & (offset_gap < window) & (key_at >= 0)
    scores = jnp.where(visible[:, None, None, :, :], scores, -jnp.inf)
    sink_value = sink_logit.reshape(1, kv_heads, group_size, 1, 1)
    top_score = jnp.maximum(jnp.max(scores, axis=-1, keepdims=True), sink_value)
    exponent = jnp.exp(scores - top_score)
    totals = jnp.sum(exponent, axis=-1, keepdims=True) + jnp.exp(sink_value - top_score)
    weights = (exponent / totals).astype(jnp.bfloat16)
    attended = jnp.einsum(
        "bkgqs,bskd->bqkgd", weights, value_blocks, preferred_element_type=jnp.float32
    )
    return attended.reshape(row_count, kv_heads * group_size * head_width).astype(jnp.bfloat16)


def discretize(decay_rate, rotation, log_step, in_re, in_im):
    time_step = jnp.exp(log_step)[:, None]
    lambda_re = -decay_rate
    modulus = jnp.exp(lambda_re * time_step)
    pole_re = modulus * jnp.cos(rotation * time_step)
    pole_im = modulus * jnp.sin(rotation * time_step)
    minus_one = pole_re - 1.0
    denominator = lambda_re * lambda_re + rotation * rotation
    factor_re = ((minus_one * lambda_re + pole_im * rotation) / denominator)[..., None]
    factor_im = ((pole_im * lambda_re - minus_one * rotation) / denominator)[..., None]
    drive_re = factor_re * in_re - factor_im * in_im
    drive_im = factor_re * in_im + factor_im * in_re
    return (pole_re, pole_im, drive_re, drive_im)


def chain_link(earlier, later):
    early_are, early_aim, early_bre, early_bim = earlier
    late_are, late_aim, late_bre, late_bim = later
    return (
        late_are * early_are - late_aim * early_aim,
        late_are * early_aim + late_aim * early_are,
        late_are * early_bre - late_aim * early_bim + late_bre,
        late_are * early_bim + late_aim * early_bre + late_bim,
    )


def local_states(inputs, pole_re, pole_im, drive_re, drive_im):
    row_count = inputs.shape[0]
    groups, states, group_width = drive_re.shape
    channel_values = inputs.astype(jnp.float32).reshape(row_count, groups, group_width)
    push_re = jnp.einsum(
        "tgh,gph->tgp", channel_values, drive_re, precision=lax.Precision.HIGHEST
    ).reshape(row_count, groups * states)
    push_im = jnp.einsum(
        "tgh,gph->tgp", channel_values, drive_im, precision=lax.Precision.HIGHEST
    ).reshape(row_count, groups * states)
    decay_re = jnp.broadcast_to(pole_re.reshape(1, groups * states), push_re.shape)
    decay_im = jnp.broadcast_to(pole_im.reshape(1, groups * states), push_im.shape)
    return lax.associative_scan(chain_link, (decay_re, decay_im, push_re, push_im), axis=0)


def apply_carry(running, carry_re, carry_im):
    power_re, power_im, own_re, own_im = running
    return (
        own_re + power_re * carry_re - power_im * carry_im,
        own_im + power_re * carry_im + power_im * carry_re,
    )


def read_out(inputs, state_re, state_im, out_re, out_im, skip_gain):
    row_count = inputs.shape[0]
    groups, group_width, states = out_re.shape
    grid_re = state_re.reshape(row_count, groups, states)
    grid_im = state_im.reshape(row_count, groups, states)
    summed = jnp.einsum(
        "tgp,ghp->tgh", grid_re, out_re, precision=lax.Precision.HIGHEST
    ) - jnp.einsum("tgp,ghp->tgh", grid_im, out_im, precision=lax.Precision.HIGHEST)
    summed = summed.reshape(row_count, groups * group_width) + skip_gain * inputs.astype(
        jnp.float32
    )
    return jax.nn.gelu(summed).astype(jnp.bfloat16)


def chain_in(power_re, power_im, end_re, end_im):
    identity = (
        jnp.ones_like(power_re),
        jnp.zeros_like(power_im),
        jnp.zeros_like(end_re),
        jnp.zeros_like(end_im),
    )
    before = carried_in((power_re, power_im, end_re, end_im), "sp", chain_link, identity)
    return (before[2], before[3])


def state_branch(inputs, decay_rate, rotation, log_step, in_re, in_im, out_re, out_im, skip_gain):
    pole_re, pole_im, drive_re, drive_im = discretize(decay_rate, rotation, log_step, in_re, in_im)
    running = local_states(inputs, pole_re, pole_im, drive_re, drive_im)
    carry_re, carry_im = chain_in(running[0][-1], running[1][-1], running[2][-1], running[3][-1])
    state_re, state_im = apply_carry(running, carry_re, carry_im)
    return read_out(inputs, state_re, state_im, out_re, out_im, skip_gain)


def earlier_window(key_rows, value_rows):
    joined = jnp.concatenate([key_rows, value_rows], axis=1)
    prior = passed_along(joined, "sp", 1)
    return jnp.concatenate([prior, joined], axis=0)


def make_adder(normed_cols):

    def add_pieces(carried, weight_pieces, row_start):
        updated = []
        for running_total, weight_piece in zip(carried, weight_pieces):
            product = lax.dot_general(
                normed_cols,
                weight_piece,
                (((0,), (0,)), ((), ())),
                preferred_element_type=jnp.float32,
            )
            updated.append(product)
        return tuple(updated)

    return add_pieces


def body(
    tokens,
    norm_gain,
    w_query,
    w_key,
    w_value,
    w_state_in,
    sink_logit,
    decay_rate,
    rotation,
    log_step,
    in_re,
    in_im,
    out_re,
    out_im,
    skip_gain,
    w_attn_out,
    w_state_out,
    out_gain,
):
    row_count = tokens.shape[0]
    window = WINDOW
    head_width = HEAD
    wide_tokens = tokens.astype(jnp.float32)
    normed = (
        wide_tokens
        * lax.rsqrt(jnp.mean(wide_tokens * wide_tokens, axis=-1, keepdims=True) + epsilon)
        * norm_gain
    ).astype(jnp.bfloat16)
    first_row = lax.axis_index("sp") * row_count
    positions = first_row + jnp.arange(row_count, dtype=jnp.int32)
    add_pieces = make_adder(jnp.transpose(normed))

    def empty_like(weight_shard):
        return jnp.zeros((row_count, weight_shard.shape[1]), jnp.float32)

    query_sum, key_sum, value_sum, input_sum = add_pieces(
        (empty_like(w_query), empty_like(w_key), empty_like(w_value), empty_like(w_state_in)),
        (
            lax.all_gather(w_query, "sp", axis=0, tiled=True),
            lax.all_gather(w_key, "sp", axis=0, tiled=True),
            lax.all_gather(w_value, "sp", axis=0, tiled=True),
            lax.all_gather(w_state_in, "sp", axis=0, tiled=True),
        ),
        jnp.int32(0),
    )
    queries, key_rows, value_rows = shape_heads(
        query_sum, key_sum, value_sum, positions, head_width
    )
    joined_rows = earlier_window(key_rows, value_rows)
    inputs = input_sum.astype(jnp.bfloat16)
    mixed_state = state_branch(
        inputs, decay_rate, rotation, log_step, in_re, in_im, out_re, out_im, skip_gain
    )
    kv_width = key_rows.shape[1]
    kv_heads = kv_width // head_width
    all_keys = joined_rows[:, :kv_width].reshape(window + row_count, kv_heads, head_width)
    all_values = joined_rows[:, kv_width:].reshape(window + row_count, kv_heads, head_width)
    attended = band_attention(queries, all_keys, all_values, sink_logit, first_row, window)
    attn_rows, state_rows = (
        lax.all_gather(w_attn_out, "sp", axis=1, tiled=True),
        lax.all_gather(w_state_out, "sp", axis=1, tiled=True),
    )
    projected = lax.psum_scatter(
        (
            jnp.dot(attended, attn_rows, preferred_element_type=jnp.float32)
            + jnp.dot(mixed_state, state_rows, preferred_element_type=jnp.float32)
        ).astype(jnp.bfloat16),
        "tp",
        scatter_dimension=0,
        tiled=True,
    ).astype(jnp.float32)
    row_scale = lax.rsqrt(jnp.mean(projected * projected, axis=-1, keepdims=True) + epsilon)
    return (projected * row_scale * out_gain).astype(jnp.bfloat16)


def solution(mesh):
    return jax.shard_map(
        body,
        mesh=mesh,
        in_specs=(
            P("sp", None),
            P(),
            P("sp", "tp"),
            P("sp", "tp"),
            P("sp", "tp"),
            P("sp", "tp"),
            P("tp"),
            P("tp", None),
            P("tp", None),
            P("tp"),
            P("tp", None, None),
            P("tp", None, None),
            P("tp", None, None),
            P("tp", None, None),
            P("tp"),
            P("tp", "sp"),
            P("tp", "sp"),
            P(),
        ),
        out_specs=P(("sp", "tp"), None),
        check_vma=False,
    )
```

profile of v0, /device:TPU:0, one launch (start us, length us, event | category | flops | bytes accessed | tf_op | source)
XLA Modules:
  0.0 1007.8 jit_solution(5649629984481578500)
XLA Ops:
  17.2 56.1 %all-gather.11.cloned.1.call-done = bf16[4096,256]{1,0:T(8,128)(2,1)} async-done(((bf16[256,256]{1,0:T(8,128)(2,1)}), bf16[4096,256]{1,0:T(8,128)(2,1)}) %all-gather.11.cloned.1.call-update) | async-done | bytes 2097168 | tf_op jit(solution)/shard_map/all_gather | solution.py:252
  76.1 59.2 %all-gather.13.cloned.1.call-done = bf16[4096,256]{1,0:T(8,128)(2,1)} async-done(((bf16[256,256]{1,0:T(8,128)(2,1)}), bf16[4096,256]{1,0:T(8,128)(2,1)}) %all-gather.13.cloned.1.call-update) | async-done | bytes 2097168 | tf_op jit(solution)/shard_map/all_gather | solution.py:253
  144.5 104.6 %all-gather.19.cloned.1.call-done = bf16[4096,1024]{1,0:T(8,128)(2,1)} async-done(((bf16[256,1024]{1,0:T(8,128)(2,1)}), bf16[4096,1024]{1,0:T(8,128)(2,1)}) %all-gather.19.cloned.1.call-update) | async-done | bytes 8388624 | tf_op jit(solution)/shard_map/all_gather | solution.py:254
  249.2 4.7 convolution_convert_fusion
  260.6 38.2 %slice.402 = f32[64,4096]{0,1:T(8,128)} slice(f32[128,4096]{0,1:T(8,128)S(1)} %bitcast.93), slice={[0:127:2], [0:4096:1]} | slice | bytes 2097152 | tf_op jit(solution)/shard_map/slice | solution.py:145
  298.8 41.3 %slice.405 = f32[64,4096]{0,1:T(8,128)} slice(f32[128,4096]{0,1:T(8,128)S(1)} %bitcast.94), slice={[1:128:2], [0:4096:1]} | slice | bytes 2097152 | tf_op jit(solution)/shard_map/slice | solution.py:145
  340.1 38.3 %slice.404 = f32[64,4096]{0,1:T(8,128)} slice(f32[128,4096]{0,1:T(8,128)} %bitcast.97), slice={[0:127:2], [0:4096:1]} | slice | bytes 2097152 | tf_op jit(solution)/shard_map/slice | solution.py:145
  378.4 38.9 %slice.411 = f32[64,4096]{0,1:T(8,128)} slice(f32[128,4096]{0,1:T(8,128)} %bitcast.98), slice={[1:128:2], [0:4096:1]} | slice | bytes 2097152 | tf_op jit(solution)/shard_map/slice | solution.py:145
  502.4 40.7 %slice.482 = f32[63,4096]{0,1:T(8,128)} slice(f32[128,4096]{0,1:T(8,128)S(1)} %bitcast.95), slice={[2:128:2], [0:4096:1]} | slice | bytes 2064384 | tf_op jit(solution)/shard_map/slice | solution.py:145
  543.1 50.7 %slice.500 = f32[63,4096]{0,1:T(8,128)} slice(f32[128,4096]{0,1:T(8,128)} %bitcast.99), slice={[2:128:2], [0:4096:1]} | slice | bytes 2064384 | tf_op jit(solution)/shard_map/slice | solution.py:145
  622.5 4.6 pad.223
  629.4 4.6 pad.222
  636.8 4.6 pad.220
  674.9 4.6 pad.196
  685.0 8.6 pad.229
  695.6 4.6 pad.194
  719.0 8.7 pad.228
  728.7 39.4 %all-gather.3 = f32[16,1,4096]{2,1,0:T(1,128)S(1)} all-gather(f32[1,1,4096]{2,1,0:T(1,128)S(1)} %add_bitcast_fusion), channel_id=1, replica_groups=mesh['sp'=16,'tp'=2] {'sp'}, dimensions={0}, use_global_device_ids=true | all-gather | bytes 278528 | tf_op jit(solution)/shard_map/all_gather | solution.py:15
  768.2 8.6 pad.199
  785.1 36.9 %all-gather.2 = f32[16,1,4096]{2,1,0:T(1,128)S(1)} all-gather(f32[1,1,4096]{2,1,0:T(1,128)S(1)} %add_bitcast_fusion.1), channel_id=1, replica_groups=mesh['sp'=16,'tp'=2] {'sp'}, dimensions={0}, use_global_device_ids=true | all-gather | bytes 278528 | tf_op jit(solution)/shard_map/all_gather | solution.py:15
  822.1 8.6 pad.227
  833.0 8.7 pad.226
  842.7 39.0 %all-gather.1 = f32[16,1,4096]{2,1,0:T(1,128)S(1)} all-gather(f32[1,1,4096]{2,1,0:T(1,128)S(1)} %add_bitcast_fusion.2), channel_id=1, replica_groups=mesh['sp'=16,'tp'=2] {'sp'}, dimensions={0}, use_global_device_ids=true | all-gather | bytes 278528 | tf_op jit(solution)/shard_map/all_gather | solution.py:15
  883.2 4.9 pad.224
  888.1 8.7 pad.225
  897.8 37.0 %all-gather = f32[16,1,4096]{2,1,0:T(1,128)S(1)} all-gather(f32[1,1,4096]{2,1,0:T(1,128)S(1)} %add_bitcast_fusion.3), channel_id=1, replica_groups=mesh['sp'=16,'tp'=2] {'sp'}, dimensions={0}, use_global_device_ids=true | all-gather | bytes 278528 | tf_op jit(solution)/shard_map/all_gather | solution.py:15
  935.7 15.3 %while.16 = (s32[]{:T(128)}, f32[4096]{0:T(1024)S(1)}, f32[4096]{0:T(1024)S(1)}, s32[]{:T(128)}, f32[16,4096]{1,0:T(8,128)}, /*index=5*/f32[16,4096]{1,0:T(8,128...) while((s32[]{:T(128)}, f32[4096]{0:T(1024)S(1)}, ...), condition=%wide.region_4.5_spmd.clone, body=%wide.region_3.4_spmd.clone.sunk | while | flops 49156 | bytes 262273 | solution.py:24
  951.0 9.2 multiply_add_fusion
  971.2 6.8 fusion.58
  980.4 4.8 fusion.65
  985.3 5.8 fusion
  991.1 6.2 reduce-scatter.2.cloned.1.call-done
  (482 shorter events, 254.2 us)
Async XLA Ops:
  6.5 958.7 %copy-start = (f32[64,16,64]{2,1,0:T(8,128)S(1)}, f32[64,16,64]{2,1,0:T(8,128)}, u32[]{:S(2)}) copy-start(f32[64,16,64]{2,1,0:T(8,128)} %param.32) | copy-start | bytes 786436
  6.6 66.7 %all-gather.11.cloned.1.call-start = ((), (), s32[]{:S(2)}) async-start(), calls=%async_computation.1 | async-start | bytes 2228224 | tf_op jit(solution)/shard_map/all_gather | solution.py:252
  7.3 128.0 %all-gather.13.cloned.1.call-start = ((), (), s32[]{:S(2)}) async-start(), calls=%async_computation.2 | async-start | bytes 2228224 | tf_op jit(solution)/shard_map/all_gather | solution.py:253
  8.0 241.1 %all-gather.19.cloned.1.call-start = ((), (), s32[]{:S(2)}) async-start(), calls=%async_computation.5 | async-start | bytes 8912896 | tf_op jit(solution)/shard_map/all_gather | solution.py:254
  8.8 64.5 %copy-start.101 = (f32[4096]{0:T(1024)S(1)}, f32[4096]{0:T(1024)}, u32[]{:S(2)}) copy-start(f32[4096]{0:T(1024)} %param.21) | copy-start | bytes 49156
  8.8 962.4 %all-gather.15.cloned.1.call-start = ((), (), s32[]{:S(2)}) async-start(), calls=%async_computation.3 | async-start | bytes 8912896 | tf_op jit(solution)/shard_map/all_gather | solution.py:251
  9.4 971.0 %all-gather.17.cloned.1.call-start = ((), (), s32[]{:S(2)}) async-start(), calls=%async_computation.4 | async-start | bytes 8912896 | tf_op jit(solution)/shard_map/all_gather | solution.py:272
  10.0 975.3 %all-gather.21.cloned.1.call-start = ((), (), s32[]{:S(2)}) async-start(), calls=%async_computation.6 | async-start | bytes 8912896 | tf_op jit(solution)/shard_map/all_gather | solution.py:273
  10.5 986.7 %reduce-scatter.2.cloned.1.call-start = ((), (), s32[]{:S(2)}) async-start(), calls=%async_computation.7 | async-start | bytes 1572864 | tf_op jit(solution)/shard_map/reduce_scatter | solution.py:275
  10.9 419.2 %copy-start.35 = (f32[4096]{0:T(1024)}, f32[4096]{0:T(1024)S(1)}, u32[]{:S(2)}) copy-start(f32[4096]{0:T(1024)S(1)} %broadcast_in_dim.18) | copy-start | bytes 49156
  11.0 64.9 %copy-start.61 = (f32[1,4096]{1,0:T(1,128)}, f32[1,4096]{1,0:T(1,128)S(1)}, u32[]{:S(2)}) copy-start(f32[1,4096]{1,0:T(1,128)S(1)} %broadcast_in_dim.20) | copy-start | bytes 49156
  11.1 419.1 %copy-start.38 = (f32[4096]{0:T(1024)}, f32[4096]{0:T(1024)S(1)}, u32[]{:S(2)}) copy-start(f32[4096]{0:T(1024)S(1)} %broadcast_in_dim.19) | copy-start | bytes 49156
  11.2 64.7 %copy-start.63 = (f32[1,4096]{1,0:T(1,128)}, f32[1,4096]{1,0:T(1,128)S(1)}, u32[]{:S(2)}) copy-start(f32[1,4096]{1,0:T(1,128)S(1)} %broadcast_in_dim.21) | copy-start | bytes 49156
  11.6 237.6 %copy-start.104 = (f32[128]{0:T(128)}, f32[128]{0:T(128)S(1)}, u32[]{:S(2)}) copy-start(f32[128]{0:T(128)S(1)} %add_rsqrt_fusion.1) | copy-start | bytes 1540
  16.4 120.9 %copy-start.41 = (f32[4096]{0:T(1024)}, f32[4096]{0:T(1024)S(1)}, u32[]{:S(2)}) copy-start(f32[4096]{0:T(1024)S(1)} %get-tuple-element.204) | copy-start | bytes 49156
  16.4 120.9 %copy-start.44 = (f32[4096]{0:T(1024)}, f32[4096]{0:T(1024)S(1)}, u32[]{:S(2)}) copy-start(f32[4096]{0:T(1024)S(1)} %get-tuple-element.205) | copy-start | bytes 49156
  17.2 58.7 %copy-start.65 = (f32[128,32]{0,1:T(8,128)}, f32[128,32]{0,1:T(8,128)S(1)}, u32[]{:S(2)}) copy-start(f32[128,32]{0,1:T(8,128)S(1)} %get-tuple-element.273) | copy-start | bytes 49156
  17.2 58.7 %copy-start.67 = (f32[128,32]{0,1:T(8,128)}, f32[128,32]{0,1:T(8,128)S(1)}, u32[]{:S(2)}) copy-start(f32[128,32]{0,1:T(8,128)S(1)} %get-tuple-element.274) | copy-start | bytes 49156
  75.9 61.4 %copy-start.71 = (bf16[128,4,32]{0,2,1:T(8,128)(2,1)}, bf16[128,4,32]{0,2,1:T(8,128)(2,1)S(1)}, u32[]{:S(2)}) copy-start(bf16[128,4,32]{0,2,1:T(8,128)(2,1)S(1)} %get-tuple-element.252) | copy-start | bytes 98308
  75.9 61.4 %copy-start.73 = (bf16[128,4,32]{0,2,1:T(8,128)(2,1)}, bf16[128,4,32]{0,2,1:T(8,128)(2,1)S(1)}, u32[]{:S(2)}) copy-start(bf16[128,4,32]{0,2,1:T(8,128)(2,1)S(1)} %get-tuple-element.253) | copy-start | bytes 98308
  137.4 5.7 collective-permute-start
  144.5 110.0 %copy-start.22 = (f32[64,64,16]{1,2,0:T(8,128)S(1)}, f32[64,64,16]{1,2,0:T(8,128)}, u32[]{:S(2)}) copy-start(f32[64,64,16]{1,2,0:T(8,128)} %param.30) | copy-start | bytes 786436
  543.1 50.8 %copy-start.96 = (f32[1,4096]{1,0:T(1,128)S(1)}, f32[1,4096]{1,0:T(1,128)}, u32[]{:S(2)}) copy-start(f32[1,4096]{1,0:T(1,128)} %get-tuple-element.257) | copy-start | bytes 49156
  543.1 50.9 %copy-start.57 = (f32[1,4096]{1,0:T(1,128)S(1)}, f32[1,4096]{1,0:T(1,128)}, u32[]{:S(2)}) copy-start(f32[1,4096]{1,0:T(1,128)} %get-tuple-element.194) | copy-start | bytes 49156
  543.1 50.9 %copy-start.95 = (f32[1,4096]{1,0:T(1,128)S(1)}, f32[1,4096]{1,0:T(1,128)}, u32[]{:S(2)}) copy-start(f32[1,4096]{1,0:T(1,128)} %get-tuple-element.256) | copy-start | bytes 49156
  543.1 51.0 %copy-start.32 = (f32[4,4096]{1,0:T(4,128)S(1)}, f32[4,4096]{1,0:T(4,128)}, u32[]{:S(2)}) copy-start(f32[4,4096]{1,0:T(4,128)} %pad.207) | copy-start | bytes 196612
  543.1 51.1 %copy-start.31 = (f32[4,4096]{1,0:T(4,128)S(1)}, f32[4,4096]{1,0:T(4,128)}, u32[]{:S(2)}) copy-start(f32[4,4096]{1,0:T(4,128)} %pad.205) | copy-start | bytes 196612
  543.1 51.1 %copy-start.42 = (f32[4096]{0:T(1024)S(1)}, f32[4096]{0:T(1024)}, u32[]{:S(2)}) copy-start(f32[4096]{0:T(1024)} %copy-done.41) | copy-start | bytes 49156
  543.1 51.1 %copy-start.45 = (f32[4096]{0:T(1024)S(1)}, f32[4096]{0:T(1024)}, u32[]{:S(2)}) copy-start(f32[4096]{0:T(1024)} %copy-done.44) | copy-start | bytes 49156
  543.1 51.1 %copy-start.94 = (f32[1,4096]{1,0:T(1,128)S(1)}, f32[1,4096]{1,0:T(1,128)}, u32[]{:S(2)}) copy-start(f32[1,4096]{1,0:T(1,128)} %get-tuple-element.196) | copy-start | bytes 49156
  543.1 51.3 %copy-start.93 = (f32[1,4096]{1,0:T(1,128)S(1)}, f32[1,4096]{1,0:T(1,128)}, u32[]{:S(2)}) copy-start(f32[1,4096]{1,0:T(1,128)} %get-tuple-element.195) | copy-start | bytes 49156
  888.1 62.8 %copy-start.8 = (f32[128,4096]{1,0:T(8,128)S(1)}, f32[128,4096]{1,0:T(8,128)}, u32[]{:S(2)}) copy-start(f32[128,4096]{1,0:T(8,128)} %pad.229) | copy-start | bytes 6291460
  (84 other events, 585.4 us)
Sparse Core Ops, SparseCore 0:
  10.1 63.0 all-gather.10
  76.0 59.1 all-gather.12
  138.0 111.0 all-gather.18
  251.8 110.4 all-gather.14
  364.8 132.6 all-gather.16
  500.1 132.6 all-gather.20
  991.2 6.0 reduce-scatter.1
where the time goes:
time: 1020 us; the launch traced here: 1010 us
  local copies, waits for them, and re-layouts  469 us (46%)
  waiting for transfers between devices  231 us (23%)
  blocking collectives  152 us (15%)
  other arithmetic  96.5 us (9%)
  matrix products  40 us (4%)
  between operations  15.5 us (2%)
    slice x47, local copies, waits for them, and re-layouts, local_states(): lax.associative_scan(chain_link, (decay_re, decay_im, push_re, push_im),...  306 us
    all_gather x4, blocking collectives, carried_in(): pieces = jax.tree.map(lambda part: lax.all_gather(part, axis), value)  152 us
    pad x48, local copies, waits for them, and re-layouts, local_states(): lax.associative_scan(chain_link, (decay_re, decay_im, push_re, push_im),...  118 us
    all_gather x1, waiting for transfers between devices, body(): lax.all_gather(w_state_in, 'sp', axis=0, tiled=True)  105 us
    all_gather x1, waiting for transfers between devices, body(): lax.all_gather(w_value, 'sp', axis=0, tiled=True)  59.2 us
    all_gather x1, waiting for transfers between devices, body(): lax.all_gather(w_key, 'sp', axis=0, tiled=True)  56.1 us
    add x12, other arithmetic, chain_link(): late_are * early_bim + late_aim * early_bre + late_bim  22.2 us
    add x23, other arithmetic, local_states(): lax.associative_scan(chain_link, (decay_re, decay_im, push_re, push_im),...  21.6 us
  transfers between devices with their start and end apart: 8, of which 5 were waited for; matrix products, arithmetic and copies ran while one was open for 59% of the time, Pallas kernels for 0%

commit v1 on v0

--- a/solution.py
+++ b/solution.py
@@ -249,7 +249,9 @@
         (empty_like(w_query), empty_like(w_key), empty_like(w_value), empty_like(w_state_in)),
         (
             lax.all_gather(w_query, "sp", axis=0, tiled=True),
-            lax.all_gather(w_key, "sp", axis=0, tiled=True),
+            jnp.concatenate(
+                lax.all_to_all(jnp.stack([w_key] * lax.axis_size("sp")), "sp", 0, 0), axis=0
+            ),
             lax.all_gather(w_value, "sp", axis=0, tiled=True),
             lax.all_gather(w_state_in, "sp", axis=0, tiled=True),
         ),

time: 1020 us -> 974 us (0.955)
  waiting for transfers between devices: 231 us -> 169 us
    all_gather x1 -> x0, waiting for transfers between devices: 56.1 us -> none  [body(): lax.all_gather(w_key, 'sp', axis=0, tiled=True)]
    all_gather x1, waiting for transfers between devices: 59.2 us -> 10.5 us  [body(): lax.all_gather(w_value, 'sp', axis=0, tiled=True)]
    all_to_all x0 -> x1, waiting for transfers between devices: none -> 42.6 us  [body(): lax.all_to_all(jnp.stack([w_key] * lax.axis_size('sp')), 'sp', 0, 0)]
    unnamed x226 -> x227, local copies, waits for them, and re-layouts: 21.5 us -> 22.6 us
  transfers between devices with their start and end apart: 8 -> 8, of which waited for: 5 -> 5; matrix products, arithmetic and copies ran while one was open for 59% -> 63% of each run, Pallas kernels for 0% -> 0%
where the time goes in v1:
time: 974 us; the launch traced here: 963 us
  local copies, waits for them, and re-layouts  477 us (49%)
  waiting for transfers between devices  169 us (17%)
  blocking collectives  152 us (16%)
  other arithmetic  97.6 us (10%)
  matrix products  39.8 us (4%)
  between operations  15.4 us (2%)
  starting transfers between devices  11.8 us (1%)
    slice x47, local copies, waits for them, and re-layouts, local_states(): lax.associative_scan(chain_link, (decay_re, decay_im, push_re, push_im),...  306 us
    all_gather x4, blocking collectives, carried_in(): pieces = jax.tree.map(lambda part: lax.all_gather(part, axis), value)  152 us
    pad x48, local copies, waits for them, and re-layouts, local_states(): lax.associative_scan(chain_link, (decay_re, decay_im, push_re, push_im),...  117 us
    all_gather x1, waiting for transfers between devices, body(): lax.all_gather(w_state_in, 'sp', axis=0, tiled=True)  105 us
    all_to_all x1, waiting for transfers between devices, body(): lax.all_to_all(jnp.stack([w_key] * lax.axis_size('sp')), 'sp', 0, 0)  42.6 us
    unnamed x227, local copies, waits for them, and re-layouts  22.6 us
    add x12, other arithmetic, chain_link(): late_are * early_bim + late_aim * early_bre + late_bim  22.3 us
    add x23, other arithmetic, local_states(): lax.associative_scan(chain_link, (decay_re, decay_im, push_re, push_im),...  21.5 us
  transfers between devices with their start and end apart: 8, of which 5 were waited for; matrix products, arithmetic and copies ran while one was open for 63% of the time, Pallas kernels for 0%

profile of v1, /device:TPU:0, one launch (start us, length us, event | category | flops | bytes accessed | tf_op | source)
XLA Modules:
  0.0 963.0 jit_solution(10053569948290447684)
XLA Ops:
  11.9 8.5 all-to-all-start
  28.8 42.6 %all-to-all-done = bf16[16,256,256]{1,2,0:T(8,128)(2,1)S(1)} async-done(((bf16[16,256,256]{1,2,0:T(8,128)(2,1)}), bf16[16,256,256]{1,2,0:T(8,128)(2,1)S(1)}, u32[]{:S(2)}, u32[]{:S(2)}) %all-to-all-start) | async-done | bytes 2097184 | tf_op jit(solution)/shard_map/all_to_all | solution.py:253
  80.7 10.5 %all-gather.10.cloned.1.call-done = bf16[4096,256]{1,0:T(8,128)(2,1)} async-done(((bf16[256,256]{1,0:T(8,128)(2,1)}), bf16[4096,256]{1,0:T(8,128)(2,1)}) %all-gather.10.cloned.1.call-update) | async-done | bytes 2097168 | tf_op jit(solution)/shard_map/all_gather | solution.py:255
  100.4 104.9 %all-gather.16.cloned.1.call-done = bf16[4096,1024]{1,0:T(8,128)(2,1)} async-done(((bf16[256,1024]{1,0:T(8,128)(2,1)}), bf16[4096,1024]{1,0:T(8,128)(2,1)}) %all-gather.16.cloned.1.call-update) | async-done | bytes 8388624 | tf_op jit(solution)/shard_map/all_gather | solution.py:256
  205.3 4.7 convolution_convert_fusion
  216.7 38.2 %slice.402 = f32[64,4096]{0,1:T(8,128)} slice(f32[128,4096]{0,1:T(8,128)S(1)} %bitcast.99), slice={[0:127:2], [0:4096:1]} | slice | bytes 2097152 | tf_op jit(solution)/shard_map/slice | solution.py:145
  255.0 41.3 %slice.405 = f32[64,4096]{0,1:T(8,128)} slice(f32[128,4096]{0,1:T(8,128)S(1)} %bitcast.100), slice={[1:128:2], [0:4096:1]} | slice | bytes 2097152 | tf_op jit(solution)/shard_map/slice | solution.py:145
  296.2 38.3 %slice.404 = f32[64,4096]{0,1:T(8,128)} slice(f32[128,4096]{0,1:T(8,128)} %bitcast.103), slice={[0:127:2], [0:4096:1]} | slice | bytes 2097152 | tf_op jit(solution)/shard_map/slice | solution.py:145
  334.5 38.9 %slice.411 = f32[64,4096]{0,1:T(8,128)} slice(f32[128,4096]{0,1:T(8,128)} %bitcast.104), slice={[1:128:2], [0:4096:1]} | slice | bytes 2097152 | tf_op jit(solution)/shard_map/slice | solution.py:145
  458.0 40.7 %slice.482 = f32[63,4096]{0,1:T(8,128)} slice(f32[128,4096]{0,1:T(8,128)S(1)} %bitcast.101), slice={[2:128:2], [0:4096:1]} | slice | bytes 2064384 | tf_op jit(solution)/shard_map/slice | solution.py:145
  498.8 50.7 %slice.500 = f32[63,4096]{0,1:T(8,128)} slice(f32[128,4096]{0,1:T(8,128)} %bitcast.105), slice={[2:128:2], [0:4096:1]} | slice | bytes 2064384 | tf_op jit(solution)/shard_map/slice | solution.py:145
  578.1 4.7 pad.223
  585.1 4.6 pad.222
  592.5 4.6 pad.220
  640.5 8.6 pad.229
  651.1 4.6 pad.194
  674.5 8.6 pad.228
  684.1 39.3 %all-gather.3 = f32[16,1,4096]{2,1,0:T(1,128)S(1)} all-gather(f32[1,1,4096]{2,1,0:T(1,128)S(1)} %add_bitcast_fusion), channel_id=1, replica_groups=mesh['sp'=16,'tp'=2] {'sp'}, dimensions={0}, use_global_device_ids=true | all-gather | bytes 278528 | tf_op jit(solution)/shard_map/all_gather | solution.py:15
  723.6 8.6 pad.199
  740.5 36.9 %all-gather.2 = f32[16,1,4096]{2,1,0:T(1,128)S(1)} all-gather(f32[1,1,4096]{2,1,0:T(1,128)S(1)} %add_bitcast_fusion.1), channel_id=1, replica_groups=mesh['sp'=16,'tp'=2] {'sp'}, dimensions={0}, use_global_device_ids=true | all-gather | bytes 278528 | tf_op jit(solution)/shard_map/all_gather | solution.py:15
  777.5 8.6 pad.227
  788.4 8.7 pad.226
  798.1 38.9 %all-gather.1 = f32[16,1,4096]{2,1,0:T(1,128)S(1)} all-gather(f32[1,1,4096]{2,1,0:T(1,128)S(1)} %add_bitcast_fusion.2), channel_id=1, replica_groups=mesh['sp'=16,'tp'=2] {'sp'}, dimensions={0}, use_global_device_ids=true | all-gather | bytes 278528 | tf_op jit(solution)/shard_map/all_gather | solution.py:15
  838.5 4.8 pad.224
  843.3 8.7 pad.225
  853.0 36.9 %all-gather = f32[16,1,4096]{2,1,0:T(1,128)S(1)} all-gather(f32[1,1,4096]{2,1,0:T(1,128)S(1)} %add_bitcast_fusion.3), channel_id=1, replica_groups=mesh['sp'=16,'tp'=2] {'sp'}, dimensions={0}, use_global_device_ids=true | all-gather | bytes 278528 | tf_op jit(solution)/shard_map/all_gather | solution.py:15
  890.8 15.3 %while.16 = (s32[]{:T(128)}, f32[4096]{0:T(1024)S(1)}, f32[4096]{0:T(1024)S(1)}, s32[]{:T(128)}, f32[16,4096]{1,0:T(8,128)}, /*index=5*/f32[16,4096]{1,0:T(8,128...) while((s32[]{:T(128)}, f32[4096]{0:T(1024)S(1)}, ...), condition=%wide.region_4.5_spmd.clone, body=%wide.region_3.4_spmd.clone.sunk | while | flops 49156 | bytes 262273 | solution.py:24
  906.1 9.2 multiply_add_fusion
  926.4 6.8 fusion.60
  935.5 4.8 fusion.66
  940.4 5.8 fusion
  946.2 6.2 reduce-scatter.2.cloned.1.call-done
  (485 shorter events, 267.7 us)
Async XLA Ops:
  6.5 913.9 %copy-start = (f32[64,16,64]{2,1,0:T(8,128)S(1)}, f32[64,16,64]{2,1,0:T(8,128)}, u32[]{:S(2)}) copy-start(f32[64,16,64]{2,1,0:T(8,128)} %param.32) | copy-start | bytes 786436
  6.5 84.7 %all-gather.10.cloned.1.call-start = ((), (), s32[]{:S(2)}) async-start(), calls=%async_computation.2 | async-start | bytes 2228224 | tf_op jit(solution)/shard_map/all_gather | solution.py:255
  7.3 198.0 %all-gather.16.cloned.1.call-start = ((), (), s32[]{:S(2)}) async-start(), calls=%async_computation.5 | async-start | bytes 8912896 | tf_op jit(solution)/shard_map/all_gather | solution.py:256
  8.0 918.3 %all-gather.12.cloned.1.call-start = ((), (), s32[]{:S(2)}) async-start(), calls=%async_computation.3 | async-start | bytes 8912896 | tf_op jit(solution)/shard_map/all_gather | solution.py:251
  8.7 926.8 %all-gather.14.cloned.1.call-start = ((), (), s32[]{:S(2)}) async-start(), calls=%async_computation.4 | async-start | bytes 8912896 | tf_op jit(solution)/shard_map/all_gather | solution.py:274
  11.9 59.6 %all-to-all-start = ((bf16[16,256,256]{1,2,0:T(8,128)(2,1)}), bf16[16,256,256]{1,2,0:T(8,128)(2,1)S(1)}, u32[]{:S(2)}, u32[]{:S(2)}) async-start(bf16[16,256,256]{1,2,0:T(8,128)(2,1)} %stack.2), calls=%async_computation | async-start | bytes 4194304 | tf_op jit(solution)/shard_map/all_to_all | solution.py:253
  20.4 920.0 %all-gather.18.cloned.1.call-start = ((), (), s32[]{:S(2)}) async-start(), calls=%async_computation.6 | async-start | bytes 8912896 | tf_op jit(solution)/shard_map/all_gather | solution.py:275
  20.9 931.5 %reduce-scatter.2.cloned.1.call-start = ((), (), s32[]{:S(2)}) async-start(), calls=%async_computation.7 | async-start | bytes 1572864 | tf_op jit(solution)/shard_map/reduce_scatter | solution.py:277
  21.3 364.9 %copy-start.35 = (f32[4096]{0:T(1024)}, f32[4096]{0:T(1024)S(1)}, u32[]{:S(2)}) copy-start(f32[4096]{0:T(1024)S(1)} %broadcast_in_dim.18) | copy-start | bytes 49156
  21.4 52.4 %copy-start.61 = (f32[1,4096]{1,0:T(1,128)}, f32[1,4096]{1,0:T(1,128)S(1)}, u32[]{:S(2)}) copy-start(f32[1,4096]{1,0:T(1,128)S(1)} %broadcast_in_dim.20) | copy-start | bytes 49156
  21.5 364.8 %copy-start.38 = (f32[4096]{0:T(1024)}, f32[4096]{0:T(1024)S(1)}, u32[]{:S(2)}) copy-start(f32[4096]{0:T(1024)S(1)} %broadcast_in_dim.19) | copy-start | bytes 49156
  21.6 52.2 %copy-start.63 = (f32[1,4096]{1,0:T(1,128)}, f32[1,4096]{1,0:T(1,128)S(1)}, u32[]{:S(2)}) copy-start(f32[1,4096]{1,0:T(1,128)S(1)} %broadcast_in_dim.21) | copy-start | bytes 49156
  27.4 177.9 %copy-start.104 = (f32[128]{0:T(128)}, f32[128]{0:T(128)S(1)}, u32[]{:S(2)}) copy-start(f32[128]{0:T(128)S(1)} %add_rsqrt_fusion.1) | copy-start | bytes 1540
  27.6 53.0 %copy-start.65 = (f32[128,32]{0,1:T(8,128)}, f32[128,32]{0,1:T(8,128)S(1)}, u32[]{:S(2)}) copy-start(f32[128,32]{0,1:T(8,128)S(1)} %get-tuple-element.273) | copy-start | bytes 49156
  27.6 53.0 %copy-start.67 = (f32[128,32]{0,1:T(8,128)}, f32[128,32]{0,1:T(8,128)S(1)}, u32[]{:S(2)}) copy-start(f32[128,32]{0,1:T(8,128)S(1)} %get-tuple-element.274) | copy-start | bytes 49156
  93.4 5.6 collective-permute-start
  100.4 110.2 %copy-start.22 = (f32[64,64,16]{1,2,0:T(8,128)S(1)}, f32[64,64,16]{1,2,0:T(8,128)}, u32[]{:S(2)}) copy-start(f32[64,64,16]{1,2,0:T(8,128)} %param.30) | copy-start | bytes 786436
  498.7 50.8 %copy-start.58 = (f32[1,4096]{1,0:T(1,128)S(1)}, f32[1,4096]{1,0:T(1,128)}, u32[]{:S(2)}) copy-start(f32[1,4096]{1,0:T(1,128)} %get-tuple-element.193) | copy-start | bytes 49156
  498.7 50.8 %copy-start.96 = (f32[1,4096]{1,0:T(1,128)S(1)}, f32[1,4096]{1,0:T(1,128)}, u32[]{:S(2)}) copy-start(f32[1,4096]{1,0:T(1,128)} %get-tuple-element.257) | copy-start | bytes 49156
  498.7 50.9 %copy-start.57 = (f32[1,4096]{1,0:T(1,128)S(1)}, f32[1,4096]{1,0:T(1,128)}, u32[]{:S(2)}) copy-start(f32[1,4096]{1,0:T(1,128)} %get-tuple-element.194) | copy-start | bytes 49156
  498.7 50.9 %copy-start.95 = (f32[1,4096]{1,0:T(1,128)S(1)}, f32[1,4096]{1,0:T(1,128)}, u32[]{:S(2)}) copy-start(f32[1,4096]{1,0:T(1,128)} %get-tuple-element.256) | copy-start | bytes 49156
  498.7 51.0 %copy-start.31 = (f32[4,4096]{1,0:T(4,128)S(1)}, f32[4,4096]{1,0:T(4,128)}, u32[]{:S(2)}) copy-start(f32[4,4096]{1,0:T(4,128)} %pad.207) | copy-start | bytes 196612
  498.7 51.0 %copy-start.32 = (f32[4,4096]{1,0:T(4,128)S(1)}, f32[4,4096]{1,0:T(4,128)}, u32[]{:S(2)}) copy-start(f32[4,4096]{1,0:T(4,128)} %pad.205) | copy-start | bytes 196612
  498.8 51.0 %copy-start.42 = (f32[4096]{0:T(1024)S(1)}, f32[4096]{0:T(1024)}, u32[]{:S(2)}) copy-start(f32[4096]{0:T(1024)} %copy-done.41) | copy-start | bytes 49156
  498.8 51.0 %copy-start.45 = (f32[4096]{0:T(1024)S(1)}, f32[4096]{0:T(1024)}, u32[]{:S(2)}) copy-start(f32[4096]{0:T(1024)} %copy-done.44) | copy-start | bytes 49156
  498.8 51.1 %copy-start.94 = (f32[1,4096]{1,0:T(1,128)S(1)}, f32[1,4096]{1,0:T(1,128)}, u32[]{:S(2)}) copy-start(f32[1,4096]{1,0:T(1,128)} %get-tuple-element.196) | copy-start | bytes 49156
  498.8 51.3 %copy-start.93 = (f32[1,4096]{1,0:T(1,128)S(1)}, f32[1,4096]{1,0:T(1,128)}, u32[]{:S(2)}) copy-start(f32[1,4096]{1,0:T(1,128)} %get-tuple-element.195) | copy-start | bytes 49156
  739.4 49.0 %copy-start.9 = (f32[128,4096]{1,0:T(8,128)}, f32[128,4096]{1,0:T(8,128)S(1)}, u32[]{:S(2)}) copy-start(f32[128,4096]{1,0:T(8,128)S(1)} %pad.198) | copy-start | bytes 6291460
  739.4 46.8 %copy-start.64 = (f32[1,4096]{1,0:T(1,128)S(1)}, f32[1,4096]{1,0:T(1,128)}, u32[]{:S(2)}) copy-start(f32[1,4096]{1,0:T(1,128)} %copy-done.63) | copy-start | bytes 49156
  788.4 48.7 %copy-start.62 = (f32[1,4096]{1,0:T(1,128)S(1)}, f32[1,4096]{1,0:T(1,128)}, u32[]{:S(2)}) copy-start(f32[1,4096]{1,0:T(1,128)} %copy-done.61) | copy-start | bytes 49156
  843.3 47.5 %copy-start.30 = (f32[4096]{0:T(1024)S(1)}, f32[4096]{0:T(1024)}, u32[]{:S(2)}) copy-start(f32[4096]{0:T(1024)} %custom-call.1) | copy-start | bytes 49156
  843.3 62.8 %copy-start.8 = (f32[128,4096]{1,0:T(8,128)S(1)}, f32[128,4096]{1,0:T(8,128)}, u32[]{:S(2)}) copy-start(f32[128,4096]{1,0:T(8,128)} %pad.229) | copy-start | bytes 6291460
  (84 other events, 489.0 us)
Sparse Core Ops, SparseCore 0:
  10.1 81.1 all-gather.9
  94.0 111.2 all-gather.15
  208.1 110.4 all-gather.11
  321.2 132.6 all-gather.13
  456.4 132.9 all-gather.17
  946.3 6.0 reduce-scatter.1
